TPU v7x, 32 devices: a whole 2x2x4 slice. The times are simulated.
32 devices in a mesh: sp: 8 (over z, y), tp: 4 (over x, core).
Axes of the slice: x: 2, y: 2, z: 4, core: 2. Of those that a mesh axis runs over, the one named last changes fastest.
Arguments:
- tokens: bfloat16 [3072, 2048], P(('sp', 'tp')), may hold values from -8 to 8, as said below
- query_weight: bfloat16 [2048, 1024], P(None, 'tp'), as said below
- key_weight: bfloat16 [2048, 256], P(None, 'tp'), as said below
- value_weight: bfloat16 [2048, 256], P(None, 'tp'), may hold values from -0.125 to 0.125
- out_weight: bfloat16 [1024, 2048], P('tp'), may hold values from -0.75 to 0.75
- query_gain: bfloat16 [16, 64], P('tp'), may hold values from 0.5 to 6.5
- key_gain: bfloat16 [4, 64], P('tp'), may hold values from 0.5 to 6.5
Outputs:
- mixed: bfloat16 [3072, 2048], P(('sp', 'tp'))
- log_sums: float32 [16, 3072], P('tp', 'sp')
Inputs may be any that keep to these rules, and one draw needn't show every extreme that they name: Each block of 384 consecutive tokens has a mean vector of its own. `query_weight`: entries are those of a weight over 2048 inputs, of magnitude at most 6 / sqrt(2048). `key_weight`: entries are those of a weight over 2048 inputs, of magnitude at most 6 / sqrt(2048).
All inputs are finite; a program needn't handle non-finite values.
Results may differ from a plain program's by a relative error of at most 0.028.
Values may be sent and summed in bfloat16 or wider, within the bound.
A program may use at most 64 MiB of HBM per device.

v0:
```python
import math

import jax
import jax.numpy as jnp
from jax import lax
from jax.sharding import PartitionSpec as P

GRID_W = 64


ROPE_BASE = 10000.0


def angle_tables(first, count, quarter):
    place = first + jnp.arange(count, dtype=jnp.int32)
    grid_row = (place // GRID_W).astype(jnp.float32)
    grid_col = (place % GRID_W).astype(jnp.float32)
    freq = ROPE_BASE ** (-jnp.arange(quarter, dtype=jnp.float32) / quarter)
    row_angle = grid_row[:, None] * freq[None, :]
    col_angle = grid_col[:, None] * freq[None, :]
    return (jnp.cos(row_angle), jnp.sin(row_angle), jnp.cos(col_angle), jnp.sin(col_angle))


def turn_pairs(part, cosine, sine):
    quarter = part.shape[-1] // 2
    first = part[..., :quarter]
    second = part[..., quarter:]
    cosine = cosine[:, None, :]
    sine = sine[:, None, :]
    return jnp.concatenate(
        [first * cosine - second * sine, second * cosine + first * sine], axis=-1
    )


def prepare(raw, gain, first):
    count = raw.shape[0]
    heads, width = gain.shape
    values = raw.astype(jnp.float32).reshape(count, heads, width)
    scaled = values * lax.rsqrt(jnp.mean(values * values, axis=-1, keepdims=True) + 1e-06)
    scaled = scaled * gain.astype(jnp.float32)[None, :, :]
    row_cos, row_sin, col_cos, col_sin = angle_tables(first, count, width // 4)
    half = width // 2
    turned = jnp.concatenate(
        [
            turn_pairs(scaled[..., :half], row_cos, row_sin),
            turn_pairs(scaled[..., half:], col_cos, col_sin),
        ],
        axis=-1,
    )
    return turned.astype(jnp.bfloat16)


def group_queries(queries, kv_count):
    count, heads, width = queries.shape
    share = heads // kv_count
    grouped = queries.reshape(count, kv_count, share, width).transpose(1, 0, 2, 3)
    return grouped.reshape(kv_count, count * share, width)


def start_state(kv_count, query_rows, width):
    top = jnp.full((kv_count, query_rows), -1e30, jnp.float32)
    total = jnp.zeros((kv_count, query_rows), jnp.float32)
    summed = jnp.zeros((kv_count, query_rows, width), jnp.float32)
    return (top, total, summed)


def fold_keys(state, pieces, grouped, scale):
    keys, values = pieces
    count, kv_count, width = keys.shape
    block_len = math.gcd(count, 1024)
    key_blocks = keys.reshape(count // block_len, block_len, kv_count, width)
    value_blocks = values.reshape(count // block_len, block_len, kv_count, width)

    def inner(carry, block):
        top, total, summed = carry
        key_block, value_block = block
        scores = (
            lax.dot_general(
                grouped, key_block, (((2,), (2,)), ((0,), (1,))), preferred_element_type=jnp.float32
            )
            * scale
        )
        new_top = jnp.maximum(top, jnp.max(scores, axis=-1))
        factor = jnp.exp(top - new_top)
        expo = jnp.exp(scores - new_top[..., None])
        total = total * factor + jnp.sum(expo, axis=-1)
        mixed = lax.dot_general(
            expo.astype(jnp.bfloat16),
            value_block,
            (((2,), (0,)), ((0,), (1,))),
            preferred_element_type=jnp.float32,
        )
        summed = summed * factor[..., None] + mixed
        return ((new_top, total, summed), None)

    state, _ = lax.scan(inner, state, (key_blocks, value_blocks))
    return state


def finish(state, count, share):
    top, total, summed = state
    kv_count, query_rows, width = summed.shape
    attended = (summed / total[..., None]).astype(jnp.bfloat16)
    attended = attended.reshape(kv_count, count, share, width).transpose(1, 0, 2, 3)
    attended = attended.reshape(count, kv_count * share * width)
    log_rows = (top + jnp.log(total)).reshape(kv_count, count, share).transpose(0, 2, 1)
    return (attended, log_rows.reshape(kv_count * share, count))


def group_project(attended, weight, groups):
    count = attended.shape[0]
    split_rows = attended.reshape(count, groups, attended.shape[1] // groups)
    split_weight = weight.reshape(groups, weight.shape[0] // groups, weight.shape[1])
    pieces = jnp.einsum(
        "ngk,gkd->gnd", split_rows, split_weight, preferred_element_type=jnp.float32
    )
    return jnp.sum(pieces.astype(jnp.bfloat16).astype(jnp.float32), axis=0).astype(jnp.bfloat16)


def body(tokens, query_weight, key_weight, value_weight, out_weight, query_gain, key_gain):
    width = query_gain.shape[1]
    scale = width ** (-0.5)
    query_cols = query_weight.shape[1]
    key_cols = key_weight.shape[1]
    kv_count = key_gain.shape[0]
    share = query_gain.shape[0] // kv_count
    piece = lax.all_gather(tokens, "tp", axis=0, tiled=True)
    made = [
        jnp.dot(piece, weight, preferred_element_type=jnp.float32).astype(jnp.bfloat16)
        for weight in (query_weight, key_weight, value_weight)
    ]
    joined = jnp.concatenate(made, axis=1)
    count = joined.shape[0]
    first = lax.axis_index("sp") * count
    queries = prepare(joined[:, :query_cols], query_gain, first)
    keys = prepare(joined[:, query_cols : query_cols + key_cols], key_gain, first)
    values = joined[:, query_cols + key_cols :].reshape(count, kv_count, width)
    grouped = group_queries(queries, kv_count)
    state = fold_keys(
        start_state(kv_count, count * share, width),
        (
            lax.all_gather(keys, "sp", axis=0, tiled=True),
            lax.all_gather(values, "sp", axis=0, tiled=True),
        ),
        grouped=grouped,
        scale=scale,
    )
    attended, log_sums = finish(state, count, share)
    whole_out = lax.all_gather(out_weight, "tp", axis=0, tiled=True)
    own_rows = lax.all_to_all(attended, "tp", split_axis=0, concat_axis=1, tiled=True)
    mixed = group_project(own_rows, whole_out, lax.axis_size("tp"))
    return (mixed, log_sums)


def solution(mesh):
    return jax.shard_map(
        body,
        mesh=mesh,
        in_specs=(
            P(("sp", "tp"), None),
            P(None, "tp"),
            P(None, "tp"),
            P(None, "tp"),
            P("tp", None),
            P("tp", None),
            P("tp", None),
        ),
        out_specs=(P(("sp", "tp"), None), P("tp", "sp")),
        check_vma=False,
    )
```

profile of v0, /device:TPU:0, one launch (start us, length us, event | category | flops | bytes accessed | tf_op | source)
XLA Modules:
  0.0 155.3 jit_solution(18443922903356023249)
XLA Ops:
  7.2 0.7 all-gather.4.cloned.1.call-update
  8.0 0.7 all-gather.6.cloned.1.call-update
  8.8 0.7 convert_element_type.68
  9.4 1.2 bitcast_convert_fusion
  10.6 0.9 multiply_cosine_fusion.1
  11.5 20.5 %all-gather.4.cloned.1.call-done = bf16[384,2048]{1,0:T(8,128)(2,1)} async-done(((bf16[96,2048]{1,0:T(8,128)(2,1)}), bf16[384,2048]{1,0:T(8,128)(2,1)}) %all-gather.4.cloned.1.call-update) | async-done | bytes 1572880 | tf_op jit(solution)/shard_map/all_gather | solution.py:127
  31.9 2.3 %fusion.24 = (f32[384,4]{0,1:T(4,128)S(1)}, bf16[384,256]{0,1:T(8,128)(2,1)S(1)}) fusion(bf16[384,2048]{1,0:T(8,128)(2,1)} %all-gather.4.cloned.1.call-done, bf16[2048,256]{1,0:T(8,128)(2,1)S(1)} %copy-done), kind=kOutput, calls=%fused_computation.32 | convolution fusion | flops 403044864 | bytes 2824192 | tf_op jit(solution)/shard_map/dot_general | solution.py:129
  34.4 0.8 subtract_convert_fusion.1
  35.2 1.0 copy.16
  36.2 1.0 copy.17
  37.2 1.0 copy.18
  38.1 1.0 copy.19
  39.1 0.6 multiply_reduce_fusion.1
  40.1 31.1 %all_gather.13 = bf16[3072,1,64]{0,2,1:T(8,128)(2,1)S(1)} all-gather(bf16[384,1,64]{0,2,1:T(8,128)(2,1)S(1)} %pad_maximum_fusion.1), channel_id=1, replica_groups=mesh['sp'=8,'tp'=4] {'sp'}, dimensions={0}, use_global_device_ids=true | all-gather | bytes 442368 | tf_op jit(solution)/shard_map/all_gather | solution.py:142
  71.3 1.5 convolution_convert_fusion.2
  72.8 31.1 %all-gather = bf16[3072,64]{0,1:T(8,128)(2,1)S(1)} all-gather(bf16[384,64]{0,1:T(8,128)(2,1)S(1)} %convolution_convert_fusion.2), channel_id=2, replica_groups=mesh['sp'=8,'tp'=4] {'sp'}, dimensions={0}, use_global_device_ids=true | all-gather | bytes 442368 | tf_op jit(solution)/shard_map/all_gather | solution.py:143
  104.6 1.9 %pad_maximum_fusion = bf16[1,1536,64]{2,1,0:T(8,128)(2,1)S(1)} fusion(bf16[1,1536,16]{2,1,0:T(8,128)(2,1)} %bitcast.64, bf16[1,1536,16]{2,1,0:T(8,128)(2,1)} %bitcast.63, bf16[1,1536,16]{2,1,0:T(8,128)(2,1)} %bitcast.62, bf16[1,1536,16]{2,1,0:T(8,128)(2,1)} %bitcast.61), kind=kLoop, calls=%fused_computation.35 | loop fusion | flops 786432 | bytes 393216 | tf_op jit(solution)/shard_map/concatenate | solution.py:43
  106.5 28.2 %while.15 = (s32[]{:T(128)}, f32[1,1536]{1,0:T(1,128)S(1)}, f32[1,1536]{1,0:T(1,128)S(1)}, f32[1,1536,64]{1,2,0:T(8,128)S(1)}, bf16[3,1024,1,64]{1,3,2,0:T(8,128...) while((s32[]{:T(128)}, f32[1,1536]{1,0:T(1,128)S(1)}, ...), condition=%wide.region_5.6_spmd.clone, body=%wide.region_2.5_spmd.clone.sunk | while | flops 415540224 | bytes 45590668 | solution.py:96
  106.5 3.7 %multiply_reduce_fusion.3 = (f32[1536]{0:T(1024)S(1)}, f32[1024,1536]{1,0:T(8,128)}) fusion(bf16[1,1536,64]{2,1,0:T(8,128)(2,1)S(1)} %get-tuple-element.205, bf16[3,1024,1,64]{1,3,2,0:T(8,128)(2,1)S(1)} %get-tuple-element.204, s32[]{:T(128)} %get-tuple-element.191), kind=kOutput, calls=%fused_computation.1.clone.1 | convolution fusion | flops 204470784 | bytes 6821892 | tf_op jit(solution)/shard_map/while/body/eval_jaxpr/dot_general | solution.py:78
  110.2 4.2 %fusion.66 = f32[1,1536,64]{1,2,0:T(8,128)S(1)} fusion(f32[1024,1536]{1,0:T(8,128)} %get-tuple-element.179, f32[1536]{0:T(1024)S(1)} %get-tuple-element.180, f32[1,1536,64]{1,2,0:T(8,128)S(1)} %get-tuple-element.194, f32[1536]{0:T(1024)S(1)} %get-tuple-element.181, pred[]{:T(512)S(6)} %compare.14, ...), kind=kOutput, calls=%fused_computation.6.clone.1 | convolution fusion | flops 206340096 | bytes 7225349 | tf_op jit(solution)/shard_map/while/body/eval_jaxpr/dot_general | solution.py:87
  114.8 1.1 fusion.64
  115.9 3.7 %multiply_reduce_fusion.3 = (f32[1536]{0:T(1024)S(1)}, f32[1024,1536]{1,0:T(8,128)}) fusion(bf16[1,1536,64]{2,1,0:T(8,128)(2,1)S(1)} %get-tuple-element.205, bf16[3,1024,1,64]{1,3,2,0:T(8,128)(2,1)S(1)} %get-tuple-element.204, s32[]{:T(128)} %get-tuple-element.191), kind=kOutput, calls=%fused_computation.1.clone.1 | convolution fusion | flops 204470784 | bytes 6821892 | tf_op jit(solution)/shard_map/while/body/eval_jaxpr/dot_general | solution.py:78
  119.7 4.2 %fusion.66 = f32[1,1536,64]{1,2,0:T(8,128)S(1)} fusion(f32[1024,1536]{1,0:T(8,128)} %get-tuple-element.179, f32[1536]{0:T(1024)S(1)} %get-tuple-element.180, f32[1,1536,64]{1,2,0:T(8,128)S(1)} %get-tuple-element.194, f32[1536]{0:T(1024)S(1)} %get-tuple-element.181, pred[]{:T(512)S(6)} %compare.14, ...), kind=kOutput, calls=%fused_computation.6.clone.1 | convolution fusion | flops 206340096 | bytes 7225349 | tf_op jit(solution)/shard_map/while/body/eval_jaxpr/dot_general | solution.py:87
  124.2 1.1 fusion.64
  125.3 3.7 %multiply_reduce_fusion.3 = (f32[1536]{0:T(1024)S(1)}, f32[1024,1536]{1,0:T(8,128)}) fusion(bf16[1,1536,64]{2,1,0:T(8,128)(2,1)S(1)} %get-tuple-element.205, bf16[3,1024,1,64]{1,3,2,0:T(8,128)(2,1)S(1)} %get-tuple-element.204, s32[]{:T(128)} %get-tuple-element.191), kind=kOutput, calls=%fused_computation.1.clone.1 | convolution fusion | flops 204470784 | bytes 6821892 | tf_op jit(solution)/shard_map/while/body/eval_jaxpr/dot_general | solution.py:78
  129.1 4.2 %fusion.66 = f32[1,1536,64]{1,2,0:T(8,128)S(1)} fusion(f32[1024,1536]{1,0:T(8,128)} %get-tuple-element.179, f32[1536]{0:T(1024)S(1)} %get-tuple-element.180, f32[1,1536,64]{1,2,0:T(8,128)S(1)} %get-tuple-element.194, f32[1536]{0:T(1024)S(1)} %get-tuple-element.181, pred[]{:T(512)S(6)} %compare.14, ...), kind=kOutput, calls=%fused_computation.6.clone.1 | convolution fusion | flops 206340096 | bytes 7225349 | tf_op jit(solution)/shard_map/while/body/eval_jaxpr/dot_general | solution.py:87
  133.6 1.1 fusion.64
  135.0 1.0 all_to_all.12
  136.0 3.4 %all-to-all-start = ((bf16[4,96,256]{2,1,0:T(8,128)(2,1)}), bf16[4,96,256]{2,1,0:T(8,128)(2,1)S(1)}, u32[]{:S(2)}, u32[]{:S(2)}) async-start(bf16[4,96,256]{2,1,0:T(8,128)(2,1)} %all_to_all.12), calls=%async_computation | async-start | bytes 393216 | tf_op jit(solution)/shard_map/all_to_all | solution.py:150
  139.6 0.7 copy.23
  140.3 4.4 %all-to-all-done = bf16[4,96,256]{2,1,0:T(8,128)(2,1)S(1)} async-done(((bf16[4,96,256]{2,1,0:T(8,128)(2,1)}), bf16[4,96,256]{2,1,0:T(8,128)(2,1)S(1)}, u32[]{:S(2)}, u32[]{:S(2)}) %all-to-all-start) | async-done | bytes 196640 | tf_op jit(solution)/shard_map/all_to_all | solution.py:150
  144.7 3.8 %fusion.22 = bf16[96,2048]{1,0:T(8,128)(2,1)} fusion(bf16[4,256,2048]{2,1,0:T(8,128)(2,1)} %bitcast.58, bf16[4,96,256]{2,1,0:T(8,128)(2,1)S(1)} %all-to-all-done), kind=kOutput, calls=%fused_computation.25 | convolution fusion | flops 404029440 | bytes 4784128 | tf_op jit(solution)/shard_map/ngk,gkd->gnd/dot_general | solution.py:114
  (48 shorter events, 3.1 us)
Async XLA Ops:
  7.2 24.8 %copy-start = (bf16[2048,256]{1,0:T(8,128)(2,1)S(1)}, bf16[2048,256]{1,0:T(8,128)(2,1)}, u32[]{:S(2)}) copy-start(bf16[2048,256]{1,0:T(8,128)(2,1)} %param.10) | copy-start | bytes 3145732
  7.2 31.9 %copy-start.3 = (bf16[2048,64]{0,1:T(8,128)(2,1)S(1)}, bf16[2048,64]{0,1:T(8,128)(2,1)}, u32[]{:S(2)}) copy-start(bf16[2048,64]{0,1:T(8,128)(2,1)} %param.11) | copy-start | bytes 786436
  7.2 24.8 %all-gather.4.cloned.1.call-start = ((), (), s32[]{:S(2)}) async-start(), calls=%async_computation.1 | async-start | bytes 1966080 | tf_op jit(solution)/shard_map/all_gather | solution.py:127
  7.9 136.7 %all-gather.6.cloned.1.call-start = ((), (), s32[]{:S(2)}) async-start(), calls=%async_computation.2 | async-start | bytes 5242880 | tf_op jit(solution)/shard_map/all_gather | solution.py:149
  8.7 2.8 %copy-start.4 = (f32[16]{0:T(128)}, f32[16]{0:T(128)S(1)}, u32[]{:S(2)}) copy-start(f32[16]{0:T(128)S(1)} %multiply_power_fusion) | copy-start | bytes 196
  31.9 7.1 %copy-start.2 = (bf16[384,2048]{1,0:T(8,128)(2,1)S(1)}, bf16[384,2048]{1,0:T(8,128)(2,1)}, u32[]{:S(2)}) copy-start(bf16[384,2048]{1,0:T(8,128)(2,1)} %all-gather.4.cloned.1.call-done) | copy-start | bytes 4718596
  34.4 5.3 %copy-start.6 = (f32[64]{0:T(128)S(1)}, f32[64]{0:T(128)}, u32[]{:S(2)}) copy-start(f32[64]{0:T(128)} %bitcast_convert_fusion) | copy-start | bytes 772
  34.4 5.4 %copy-start.5 = (f32[16]{0:T(128)S(1)}, f32[16]{0:T(128)}, u32[]{:S(2)}) copy-start(f32[16]{0:T(128)} %copy-done.4) | copy-start | bytes 196
  110.2 4.6 %copy-start.1 = (f32[1024,1536]{1,0:T(8,128)S(1)}, f32[1024,1536]{1,0:T(8,128)}, u32[]{:S(2)}) copy-start(f32[1024,1536]{1,0:T(8,128)} %get-tuple-element.179) | copy-start | bytes 18874372 | tf_op jit(solution)/shard_map/while
  119.6 4.6 %copy-start.1 = (f32[1024,1536]{1,0:T(8,128)S(1)}, f32[1024,1536]{1,0:T(8,128)}, u32[]{:S(2)}) copy-start(f32[1024,1536]{1,0:T(8,128)} %get-tuple-element.179) | copy-start | bytes 18874372 | tf_op jit(solution)/shard_map/while
  129.0 4.6 %copy-start.1 = (f32[1024,1536]{1,0:T(8,128)S(1)}, f32[1024,1536]{1,0:T(8,128)}, u32[]{:S(2)}) copy-start(f32[1024,1536]{1,0:T(8,128)} %get-tuple-element.179) | copy-start | bytes 18874372 | tf_op jit(solution)/shard_map/while
  136.0 8.6 %all-to-all-start = ((bf16[4,96,256]{2,1,0:T(8,128)(2,1)}), bf16[4,96,256]{2,1,0:T(8,128)(2,1)S(1)}, u32[]{:S(2)}, u32[]{:S(2)}) async-start(bf16[4,96,256]{2,1,0:T(8,128)(2,1)} %all_to_all.12), calls=%async_computation | async-start | bytes 393216 | tf_op jit(solution)/shard_map/all_to_all | solution.py:150
Sparse Core Ops, SparseCore 0:
  9.6 22.3 all-gather.3
  33.5 34.4 all-gather.5
where the time goes:
time: 156 us; the launch traced here: 155 us
  blocking collectives  62.2 us (40%)
  matrix products  31.9 us (20%)
  waiting for transfers between devices  26.2 us (17%)
  between operations  14.2 us (9%)
  other arithmetic  9.4 us (6%)
  local copies, waits for them, and re-layouts  7.79 us (5%)
  starting transfers between devices  3.44 us (2%)
    all_gather x1, blocking collectives, body(): lax.all_gather(keys, 'sp', axis=0, tiled=True)  31.1 us
    all_gather x1, blocking collectives, body(): lax.all_gather(values, 'sp', axis=0, tiled=True)  31.1 us
    all_gather x1, waiting for transfers between devices, body(): piece = lax.all_gather(tokens, 'tp', axis=0, tiled=True)  20.5 us
    dot_general x3, matrix products, inner(): lax.dot_general(expo.astype(jnp.bfloat16), value_block, (((2,), (0,)), ((...  12.6 us
    dot_general x3, matrix products, inner(): lax.dot_general(grouped, key_block, (((2,), (2,)), ((0,), (1,))), preferr...  11.1 us
    dot_general x3, matrix products, body(): jnp.dot(piece, weight, preferred_element_type=jnp.float32)  4.45 us
    all_to_all x1, waiting for transfers between devices, body(): lax.all_to_all(attended, 'tp', split_axis=0, concat_axis=1, tiled=True)  4.36 us
    another operation x4, local copies, waits for them, and re-layouts  3.87 us
  transfers between devices with their start and end apart: 3, of which 2 were waited for; matrix products, arithmetic and copies ran while one was open for 28% of the time, Pallas kernels for 0%

commit v1 on v0

v1 whole, which is shorter than its diff:
```python
import functools
import math

import jax
import jax.numpy as jnp
from jax import lax
from jax.experimental import pallas as pl
from jax.experimental.pallas import tpu as pltpu
from jax.sharding import PartitionSpec as P

GRID_W = 64
ROPE_BASE = 10000.0
EPS = 1e-06
LOG2E = math.log2(math.e)
LN2 = math.log(2.0)
ONES = 16
MESH = pl.DeviceIdType.MESH
F32 = jnp.float32
BF16 = jnp.bfloat16


def prepare(x, gain, tables):
    quarter = x.shape[0] // 4
    x = x * lax.rsqrt(jnp.mean(x * x, axis=0, keepdims=True) + EPS) * gain
    a, b, c, d = (x[i * quarter : (i + 1) * quarter] for i in range(4))
    row_cos, row_sin, col_cos, col_sin = tables
    return jnp.concatenate(
        [
            a * row_cos - b * row_sin,
            b * row_cos + a * row_sin,
            c * col_cos - d * col_sin,
            d * col_cos + c * col_sin,
        ],
        axis=0,
    )


def angle_tables(first, count, quarter):
    place = first + lax.broadcasted_iota(jnp.int32, (quarter, count), 1)
    order = lax.broadcasted_iota(jnp.int32, (quarter, count), 0).astype(F32)
    freq = jnp.exp(order * (-math.log(ROPE_BASE) / quarter))
    shift = GRID_W.bit_length() - 1
    row = lax.shift_right_logical(place, shift).astype(F32) * freq
    col = jnp.bitwise_and(place, GRID_W - 1).astype(F32) * freq
    return (jnp.cos(row), jnp.sin(row), jnp.cos(col), jnp.sin(col))


def kernel(
    n_sp,
    n_tp,
    chunks,
    tok_hbm,
    wq_hbm,
    wk_hbm,
    wv_hbm,
    wo_hbm,
    qg_ref,
    kg_ref,
    mixed_ref,
    log_ref,
    tok,
    wq,
    wk,
    wv,
    wkv,
    wo,
    gains,
    raw,
    queries,
    kv,
    top,
    acc,
    att_own,
    att_out,
    att_in,
    part_out,
    part_in,
    local_sem,
    tok_send,
    tok_recv,
    wo_send,
    wo_recv,
    kv_send,
    kv_recv,
    att_send,
    att_recv,
    part_send,
    part_recv,
):
    sp = lax.axis_index("sp")
    tp = lax.axis_index("tp")
    pairs = n_tp // 2
    cols = n_sp // 2
    pair, core = tp // 2, tp % 2
    mate = pair * 2 + (1 - core)
    col, side = sp // 2, sp % 2
    other = col * 2 + (1 - side)
    rows = tok.shape[1]
    heads, width = qg_ref.shape
    kv_heads = kg_ref.shape[0]
    share = heads // kv_heads
    count = rows * n_tp

    def across(i):
        return lax.rem(pair + i, pairs) * 2 + core

    def column(i):
        return lax.rem(col + i, cols) * 2 + side

    loads = [
        pltpu.make_async_copy(src, dst, local_sem.at[i])
        for i, (src, dst) in enumerate(
            ((tok_hbm, tok.at[tp]), (wq_hbm, wq), (wk_hbm, wk), (wv_hbm, wv), (wo_hbm, wo.at[core]))
        )
    ]
    for load in loads:
        load.start()

    barrier = pltpu.get_barrier_semaphore()
    peers = 0
    for i in range(1, pairs):
        pl.semaphore_signal(barrier, inc=1, device_id={"tp": across(i)}, device_id_type=MESH)
        peers += 1
    pl.semaphore_signal(barrier, inc=1, device_id={"tp": mate}, device_id_type=MESH)
    pl.semaphore_signal(barrier, inc=1, device_id={"sp": other}, device_id_type=MESH)
    peers += 2
    for i in range(1, cols):
        pl.semaphore_signal(barrier, inc=1, device_id={"sp": column(i)}, device_id_type=MESH)
        peers += 1
    pl.semaphore_wait(barrier, peers)

    def send(src, dst, send_sem, recv_sem, where):
        return pltpu.make_async_remote_copy(
            src_ref=src,
            dst_ref=dst,
            send_sem=send_sem,
            recv_sem=recv_sem,
            device_id=where,
            device_id_type=MESH,
        )

    pending = []

    def go(copy):
        copy.start()
        pending.append(copy)

    def token_copy(block, src, slot, target):
        return send(src, tok.at[block], tok_send.at[slot], tok_recv.at[block], {"tp": target})

    for i in range(1, pairs):
        go(token_copy(tp, tok_hbm, i, across(i)))
    go(token_copy(tp, tok_hbm, 0, mate))

    gains[...] = jnp.zeros_like(gains)
    gains[0:heads, 0:width] = qg_ref[...].astype(F32) * (LOG2E * width ** (-0.5))
    gains[heads : heads + kv_heads, 0:width] = kg_ref[...].astype(F32)
    turned_gains = jnp.transpose(gains[...])
    tables = angle_tables(sp * count, count, width // 4)
    top[...] = jnp.full_like(top, -1e30)
    acc[...] = jnp.zeros_like(acc)
    loads[2].wait()
    loads[3].wait()
    kv_cols = wk.shape[1]
    wkv[:, 0:kv_cols] = wk[...]
    wkv[:, kv_cols : 2 * kv_cols] = wv[...]
    loads[1].wait()
    loads[0].wait()
    query_cols = wq.shape[1]

    def project(block):
        piece = tok[block]
        at = pl.ds(pl.multiple_of(block * rows, rows), rows)
        raw[at, 0:query_cols] = jnp.dot(piece, wq[...], preferred_element_type=F32)
        raw[at, query_cols:] = jnp.dot(piece, wkv[...], preferred_element_type=F32)

    project(tp)
    token_copy(mate, tok_hbm, 0, mate).wait_recv()
    project(mate)
    for i in range(1, pairs):
        block = across(i)
        token_copy(block, tok_hbm, i, block).wait_recv()
        go(token_copy(block, tok.at[block], pairs + i, mate))
        project(block)
    loads[4].wait()
    wo_copy = send(wo_hbm, wo.at[core], wo_send, wo_recv, {"tp": mate})
    wo_copy.start()
    for i in range(1, pairs):
        block = lax.rem(pair + i, pairs) * 2 + (1 - core)
        token_copy(block, tok_hbm, i, mate).wait_recv()
        project(block)

    turned = jnp.transpose(raw[:, query_cols:])
    kv_rows = kv_heads * width
    for h in range(kv_heads):
        keys = prepare(
            turned[h * width : (h + 1) * width], turned_gains[0:width, heads + h : heads + h + 1], tables
        )
        kv[sp, h * width : (h + 1) * width, :] = keys.astype(BF16)
    kv[sp, kv_rows : 2 * kv_rows, :] = turned[kv_rows : 2 * kv_rows].astype(BF16)

    def kv_copy(block, slot, where):
        return send(kv.at[block], kv.at[block], kv_send.at[slot], kv_recv.at[block], {"sp": where})

    for i in range(1, cols):
        go(kv_copy(sp, i, column(i)))
    go(kv_copy(sp, 0, other))

    turned = jnp.transpose(raw[:, 0:query_cols])
    for h in range(heads):
        q = prepare(turned[h * width : (h + 1) * width], turned_gains[0:width, h : h + 1], tables)
        queries[h] = q.astype(BF16)

    def attend(block):
        ones = jnp.ones((ONES, count), BF16)
        for g in range(kv_heads):
            keys = jnp.transpose(kv[block, g * width : (g + 1) * width, :])
            values = kv[block, kv_rows + g * width : kv_rows + (g + 1) * width, :]
            values = jnp.concatenate([values, ones], axis=0)
            for h in range(g * share, (g + 1) * share):
                scores = jnp.dot(keys, queries[h], preferred_element_type=F32)
                old = top[h : h + 1, :]
                new = jnp.maximum(old, jnp.max(scores, axis=0, keepdims=True))
                weights = jnp.exp2(scores - new).astype(BF16)
                mixed = jnp.dot(values, weights, preferred_element_type=F32)
                acc[h] = acc[h] * jnp.exp2(old - new) + mixed
                top[h : h + 1, :] = new

    attend(sp)

    def step(i, carry):
        block = column(i)
        kv_copy(block, 0, block).wait_recv()
        kv_copy(block, cols + i, other).start()
        attend(block)
        late = lax.rem(col + i - 1, cols) * 2 + (1 - side)
        kv_copy(late, 0, other).wait_recv()
        attend(late)
        return carry

    lax.fori_loop(1, cols, step, 0)
    late = lax.rem(col + cols - 1, cols) * 2 + (1 - side)
    kv_copy(late, 0, other).wait_recv()
    attend(late)

    finished = []
    for h in range(heads):
        total = acc[h, width : width + 1, :]
        finished.append(acc[h, 0:width, :] / total)
        log_ref[h : h + 1, :] = (top[h : h + 1, :] + jnp.log2(total)) * LN2
    attended = jnp.transpose(jnp.concatenate(finished, axis=0)).astype(BF16)
    for t in range(n_tp):
        piece = attended[t * rows : (t + 1) * rows]

        @pl.when(core == t % 2)
        def _():
            att_own[t // 2] = piece

        @pl.when(core != t % 2)
        def _():
            att_out[t // 2] = piece

    att_copy = send(att_out, att_in, att_send, att_recv, {"tp": mate})
    att_copy.start()
    att_copy.wait_recv()
    wo_copy.wait_recv()
    step_cols = mixed_ref.shape[1] // chunks

    def product(place, n):
        at = slice(n * step_cols, (n + 1) * step_cols)
        return jnp.dot(
            att_own[place], wo[core, :, at], preferred_element_type=F32
        ) + jnp.dot(att_in[place], wo[1 - core, :, at], preferred_element_type=F32)

    def part_copy(i, n):
        slot = (i - 1) * chunks + n
        return send(
            part_out.at[slot],
            part_in.at[slot],
            part_send.at[slot],
            part_recv.at[slot],
            {"tp": across(i)},
        )

    for n in range(chunks):
        for i in range(1, pairs):
            part_out[(i - 1) * chunks + n] = product(lax.rem(pair + i, pairs), n).astype(BF16)
            part_copy(i, n).start()
    for n in range(chunks):
        at = slice(n * step_cols, (n + 1) * step_cols)
        total = product(pair, n)
        for i in range(1, pairs):
            part_copy(i, n).wait_recv()
            total = total + part_in[(i - 1) * chunks + n].astype(F32)
        mixed_ref[:, at] = total.astype(BF16)

    for copy in pending:
        copy.wait_send()
    wo_copy.wait_send()
    att_copy.wait_send()
    for i in range(1, cols):
        kv_copy(column(i), cols + i, other).wait_send()
    for n in range(chunks):
        for i in range(1, pairs):
            part_copy(i, n).wait_send()


def body(n_sp, n_tp, tokens, query_weight, key_weight, value_weight, out_weight, query_gain, key_gain):
    rows, depth = tokens.shape
    query_cols = query_weight.shape[1]
    kv_cols = key_weight.shape[1]
    heads, width = query_gain.shape
    kv_heads = key_gain.shape[0]
    group, model = out_weight.shape
    count = rows * n_tp
    pairs, cols = n_tp // 2, n_sp // 2
    chunks = 4
    any_space = pl.BlockSpec(memory_space=pl.ANY)
    vmem = pl.BlockSpec(memory_space=pltpu.VMEM)
    dma = pltpu.SemaphoreType.DMA
    slots = max(pairs - 1, 1) * chunks
    return pl.pallas_call(
        functools.partial(kernel, n_sp, n_tp, chunks),
        out_shape=(
            jax.ShapeDtypeStruct((rows, model), BF16),
            jax.ShapeDtypeStruct((heads, count), F32),
        ),
        in_specs=[any_space] * 5 + [vmem] * 2,
        out_specs=(vmem, vmem),
        scratch_shapes=[
            pltpu.VMEM((n_tp, rows, depth), BF16),
            pltpu.VMEM((depth, query_cols), BF16),
            pltpu.VMEM((depth, kv_cols), BF16),
            pltpu.VMEM((depth, kv_cols), BF16),
            pltpu.VMEM((depth, 2 * kv_cols), BF16),
            pltpu.VMEM((2, group, model), BF16),
            pltpu.VMEM((128, 128), F32),
            pltpu.VMEM((count, query_cols + 2 * kv_cols), F32),
            pltpu.VMEM((heads, width, count), BF16),
            pltpu.VMEM((n_sp, 2 * kv_heads * width, count), BF16),
            pltpu.VMEM((heads, count), F32),
            pltpu.VMEM((heads, width + ONES, count), F32),
            pltpu.VMEM((pairs, rows, group), BF16),
            pltpu.VMEM((pairs, rows, group), BF16),
            pltpu.VMEM((pairs, rows, group), BF16),
            pltpu.VMEM((slots, rows, model // chunks), BF16),
            pltpu.VMEM((slots, rows, model // chunks), BF16),
            dma((5,)),
            dma((2 * pairs,)),
            dma((n_tp,)),
            dma,
            dma,
            dma((2 * cols,)),
            dma((n_sp,)),
            dma,
            dma,
            dma((slots,)),
            dma((slots,)),
        ],
        compiler_params=pltpu.CompilerParams(
            collective_id=0, has_side_effects=True, vmem_limit_bytes=60 * 1024 * 1024
        ),
        name="attention",
    )(tokens, query_weight, key_weight, value_weight, out_weight, query_gain, key_gain)


def solution(mesh):
    return jax.shard_map(
        functools.partial(body, mesh.shape["sp"], mesh.shape["tp"]),
        mesh=mesh,
        in_specs=(
            P(("sp", "tp"), None),
            P(None, "tp"),
            P(None, "tp"),
            P(None, "tp"),
            P("tp", None),
            P("tp", None),
            P("tp", None),
        ),
        out_specs=(P(("sp", "tp"), None), P("tp", "sp")),
        check_vma=False,
    )
```

time: 156 us -> 57.1 us (0.37)
  blocking collectives: 62.2 us -> 0 us
  Pallas kernels: 0 us -> 50.3 us
  matrix products: 31.9 us -> 0 us
  waiting for transfers between devices: 26.2 us -> 0 us
  between operations: 14.2 us -> 0.66 us
  other arithmetic: 9.4 us -> 0 us
  starting transfers between devices: 3.44 us -> 0 us
  local copies, waits for them, and re-layouts: 7.79 us -> 5.37 us
    all_gather x2 -> x0, blocking collectives: 62.2 us -> none  [the longest x1 31.1 us: body(): lax.all_gather(keys, 'sp', axis=0, tiled=True)]
    pallas_call x0 -> x1, Pallas kernels: none -> 50.3 us  [body(): pl.pallas_call(functools.partial(kernel, n_sp, n_tp, chunks), out_shape=(...]
    dot_general x10 -> x0, matrix products: 31.9 us -> none  [the longest x3 12.6 us: inner(): lax.dot_general(expo.astype(jnp.bfloat16), value_block, (((2,), (0,)), ((...]
    all_gather x2 -> x0, waiting for transfers between devices: 20.5 us -> none  [the longest x1 20.5 us: body(): piece = lax.all_gather(tokens, 'tp', axis=0, tiled=True)]
    unnamed x14 -> x8, local copies, waits for them, and re-layouts: 0.89 us -> 5.37 us
    all_to_all x1 -> x0, waiting for transfers between devices: 4.36 us -> none  [body(): lax.all_to_all(attended, 'tp', split_axis=0, concat_axis=1, tiled=True)]
    another operation x4 -> x0, local copies, waits for them, and re-layouts: 3.87 us -> none
    all_to_all x1 -> x0, starting transfers between devices: 3.37 us -> none  [body(): lax.all_to_all(attended, 'tp', split_axis=0, concat_axis=1, tiled=True)]
  transfers between devices with their start and end apart: 3 -> 0, of which waited for: 2 -> 0; matrix products, arithmetic and copies ran while one was open for 28% -> 0% of each run, Pallas kernels for 0% -> 0%
where the time goes in v1:
time: 57.1 us; the launch traced here: 56.3 us
  Pallas kernels  50.3 us (88%)
  local copies, waits for them, and re-layouts  5.37 us (9%)
  between operations  0.66 us (1%)
    pallas_call x1, Pallas kernels, body(): pl.pallas_call(functools.partial(kernel, n_sp, n_tp, chunks), out_shape=(...  50.3 us
    unnamed x8, local copies, waits for them, and re-layouts  5.37 us

profile of v1, /device:TPU:0, one launch (start us, length us, event | category | flops | bytes accessed | tf_op | source)
XLA Modules:
  0.0 56.3 jit_solution(15222624854063329803)
XLA Ops:
  0.6 0.0 copy-start
  0.6 2.0 %copy.9.wk_hbm = bf16[2048,64]{1,0:T(8,128)(2,1)} copy(bf16[2048,64]{0,1:T(8,128)(2,1)} %param.9) | data formatting | bytes 524288 | tf_op args[2]
  2.6 0.0 copy-done
  2.6 1.0 %copy.10.wv_hbm = bf16[2048,64]{1,0:T(8,128)(2,1)} copy(bf16[2048,64]{0,1:T(8,128)(2,1)S(1)} %copy-done) | data formatting | bytes 524288 | tf_op args[3]
  3.6 50.3 %attention.1 = (bf16[96,2048]{1,0:T(8,128)(2,1)}, f32[4,384]{1,0:T(4,128)}) custom-call(bf16[96,2048]{1,0:T(8,128)(2,1)} %tok_hbm.1, bf16[2048,256]{1,0:T(8,128)(2,1)} %wq_hbm.1, bf16[2048,64]{1,0:T(8,128)(2,1)} %copy.9.wk_hbm, bf16[2048,64]{1,0:T(8,128)(2,1)} %copy.10.wv_hbm, bf16[256,2048]{1,0:T(8,128)(2,1)} %wo_hbm.1, bf16[4,64]{1,0:T(4,128)(2,1)} %qg_ref.1, ...), custom_call_target="tpu_custom_call" | custom-call | tf_op jit(solution)/shard_map/attention/pallas_call | solution.py:322
  54.0 0.0 copy-start.1
  54.0 1.8 %copy.13 = bf16[96,2048]{1,0:T(8,128)(2,1)} copy(bf16[96,2048]{1,0:T(8,128)(2,1)} %get-tuple-element.4) | data formatting | bytes 786432
  55.8 0.0 copy-done.1
  55.8 0.6 %copy.14 = f32[4,384]{1,0:T(4,128)} copy(f32[4,384]{1,0:T(4,128)S(1)} %copy-done.1) | data formatting | bytes 12288
Async XLA Ops:
  0.6 2.0 %copy-start = (bf16[2048,64]{0,1:T(8,128)(2,1)S(1)}, bf16[2048,64]{0,1:T(8,128)(2,1)}, u32[]{:S(2)}) copy-start(bf16[2048,64]{0,1:T(8,128)(2,1)} %param.10) | copy-start | bytes 786436
  54.0 1.8 %copy-start.1 = (f32[4,384]{1,0:T(4,128)S(1)}, f32[4,384]{1,0:T(4,128)}, u32[]{:S(2)}) copy-start(f32[4,384]{1,0:T(4,128)} %get-tuple-element.5) | copy-start | bytes 18436

commit v2 on v1

--- a/solution.py
+++ b/solution.py
@@ -60,8 +60,6 @@
     log_ref,
     tok,
     wq,
-    wk,
-    wv,
     wkv,
     wo,
     gains,
@@ -104,13 +102,11 @@
     def across(i):
         return lax.rem(pair + i, pairs) * 2 + core
 
-    def column(i):
-        return lax.rem(col + i, cols) * 2 + side
-
+    kv_cols = wk_hbm.shape[0]
     loads = [
         pltpu.make_async_copy(src, dst, local_sem.at[i])
         for i, (src, dst) in enumerate(
-            ((tok_hbm, tok.at[tp]), (wq_hbm, wq), (wk_hbm, wk), (wv_hbm, wv), (wo_hbm, wo.at[core]))
+            ((tok_hbm, tok.at[tp]), (wq_hbm, wq), (wk_hbm, wkv.at[0:kv_cols]), (wv_hbm, wkv.at[kv_cols:]), (wo_hbm, wo.at[core]))
         )
     ]
     for load in loads:
@@ -124,8 +120,9 @@
     pl.semaphore_signal(barrier, inc=1, device_id={"tp": mate}, device_id_type=MESH)
     pl.semaphore_signal(barrier, inc=1, device_id={"sp": other}, device_id_type=MESH)
     peers += 2
-    for i in range(1, cols):
-        pl.semaphore_signal(barrier, inc=1, device_id={"sp": column(i)}, device_id_type=MESH)
+    for way in (1, -1):
+        near = lax.rem(col + way + cols, cols) * 2 + side
+        pl.semaphore_signal(barrier, inc=1, device_id={"sp": near}, device_id_type=MESH)
         peers += 1
     pl.semaphore_wait(barrier, peers)
 
@@ -161,9 +158,6 @@
     acc[...] = jnp.zeros_like(acc)
     loads[2].wait()
     loads[3].wait()
-    kv_cols = wk.shape[1]
-    wkv[:, 0:kv_cols] = wk[...]
-    wkv[:, kv_cols : 2 * kv_cols] = wv[...]
     loads[1].wait()
     loads[0].wait()
     query_cols = wq.shape[1]
@@ -172,7 +166,9 @@
         piece = tok[block]
         at = pl.ds(pl.multiple_of(block * rows, rows), rows)
         raw[at, 0:query_cols] = jnp.dot(piece, wq[...], preferred_element_type=F32)
-        raw[at, query_cols:] = jnp.dot(piece, wkv[...], preferred_element_type=F32)
+        raw[at, query_cols:] = lax.dot_general(
+            piece, wkv[...], (((1,), (1,)), ((), ())), preferred_element_type=F32
+        )
 
     project(tp)
     token_copy(mate, tok_hbm, 0, mate).wait_recv()
@@ -199,12 +195,36 @@
         kv[sp, h * width : (h + 1) * width, :] = keys.astype(BF16)
     kv[sp, kv_rows : 2 * kv_rows, :] = turned[kv_rows : 2 * kv_rows].astype(BF16)
 
-    def kv_copy(block, slot, where):
-        return send(kv.at[block], kv.at[block], kv_send.at[slot], kv_recv.at[block], {"sp": where})
-
-    for i in range(1, cols):
-        go(kv_copy(sp, i, column(i)))
-    go(kv_copy(sp, 0, other))
+    half = cols // 2
+    mirror = 1 - side
+
+    def column(i):
+        return lax.rem(col + i + cols, cols)
+
+    def kv_copy(block, part, slot, where):
+        spot = kv.at[block]
+        if part is not None:
+            spot = kv.at[block, part * kv_rows : (part + 1) * kv_rows]
+        return send(spot, spot, kv_send.at[slot], kv_recv.at[block, part or 0], {"sp": where})
+
+    slots = iter(range(4 * n_sp))
+
+    def pass_on(distance, s, way):
+        if distance > half or (distance == half and s is mirror):
+            return
+        part = None if distance < half else (0 if way > 0 else 1)
+        block = column(-(distance - 1) * way) * 2 + s
+        go(kv_copy(block, part, next(slots), column(way) * 2 + side))
+
+    def landed(distance, s, way):
+        block = column(-distance * way) * 2 + s
+        part = None if distance < half else (0 if way > 0 else 1)
+        kv_copy(block, part, 0, other).wait_recv()
+        return block
+
+    go(kv_copy(sp, None, next(slots), other))
+    for way in (1, -1):
+        pass_on(1, side, way)
 
     turned = jnp.transpose(raw[:, 0:query_cols])
     for h in range(heads):
@@ -227,21 +247,38 @@
                 top[h : h + 1, :] = new
 
     attend(sp)
-
-    def step(i, carry):
-        block = column(i)
-        kv_copy(block, 0, block).wait_recv()
-        kv_copy(block, cols + i, other).start()
-        attend(block)
-        late = lax.rem(col + i - 1, cols) * 2 + (1 - side)
-        kv_copy(late, 0, other).wait_recv()
-        attend(late)
-        return carry
-
-    lax.fori_loop(1, cols, step, 0)
-    late = lax.rem(col + cols - 1, cols) * 2 + (1 - side)
-    kv_copy(late, 0, other).wait_recv()
-    attend(late)
+    kv_copy(other, None, 0, other).wait_recv()
+    for way in (1, -1):
+        pass_on(1, mirror, way)
+    attend(other)
+
+    def opposite():
+        for way in (1, -1):
+            block = landed(half, side, way)
+        go(kv_copy(block, None, next(slots), other))
+        return block
+
+    for distance in range(1, half):
+        arrived = []
+        for way in (1, -1):
+            arrived.append(landed(distance, side, way))
+            pass_on(distance + 1, side, way)
+        for block in arrived:
+            attend(block)
+        if distance == half - 1:
+            last = opposite()
+        arrived = []
+        for way in (1, -1):
+            arrived.append(landed(distance, mirror, way))
+            pass_on(distance + 1, mirror, way)
+        for block in arrived:
+            attend(block)
+    if half == 1:
+        last = opposite()
+    attend(last)
+    last = column(half) * 2 + mirror
+    kv_copy(last, None, 0, other).wait_recv()
+    attend(last)
 
     finished = []
     for h in range(heads):
@@ -298,8 +335,6 @@
         copy.wait_send()
     wo_copy.wait_send()
     att_copy.wait_send()
-    for i in range(1, cols):
-        kv_copy(column(i), cols + i, other).wait_send()
     for n in range(chunks):
         for i in range(1, pairs):
             part_copy(i, n).wait_send()
@@ -313,7 +348,7 @@
     kv_heads = key_gain.shape[0]
     group, model = out_weight.shape
     count = rows * n_tp
-    pairs, cols = n_tp // 2, n_sp // 2
+    pairs = n_tp // 2
     chunks = 4
     any_space = pl.BlockSpec(memory_space=pl.ANY)
     vmem = pl.BlockSpec(memory_space=pltpu.VMEM)
@@ -322,17 +357,15 @@
     return pl.pallas_call(
         functools.partial(kernel, n_sp, n_tp, chunks),
         out_shape=(
-            jax.ShapeDtypeStruct((rows, model), BF16),
-            jax.ShapeDtypeStruct((heads, count), F32),
+            pltpu.VMEM((rows, model), BF16),
+            pltpu.VMEM((heads, count), F32),
         ),
         in_specs=[any_space] * 5 + [vmem] * 2,
         out_specs=(vmem, vmem),
         scratch_shapes=[
             pltpu.VMEM((n_tp, rows, depth), BF16),
             pltpu.VMEM((depth, query_cols), BF16),
-            pltpu.VMEM((depth, kv_cols), BF16),
-            pltpu.VMEM((depth, kv_cols), BF16),
-            pltpu.VMEM((depth, 2 * kv_cols), BF16),
+            pltpu.VMEM((2 * kv_cols, depth), BF16),
             pltpu.VMEM((2, group, model), BF16),
             pltpu.VMEM((128, 128), F32),
             pltpu.VMEM((count, query_cols + 2 * kv_cols), F32),
@@ -350,8 +383,8 @@
             dma((n_tp,)),
             dma,
             dma,
-            dma((2 * cols,)),
-            dma((n_sp,)),
+            dma((4 * n_sp,)),
+            dma((n_sp, 2)),
             dma,
             dma,
             dma((slots,)),
@@ -361,7 +394,7 @@
             collective_id=0, has_side_effects=True, vmem_limit_bytes=60 * 1024 * 1024
         ),
         name="attention",
-    )(tokens, query_weight, key_weight, value_weight, out_weight, query_gain, key_gain)
+    )(tokens, query_weight, key_weight.T, value_weight.T, out_weight, query_gain, key_gain)
 
 
 def solution(mesh):

time: 57.1 us -> 50.3 us (0.88); the launches traced: 56.3 us -> 50.2 us
  local copies, waits for them, and re-layouts: 5.37 us -> 1.34 us
  Pallas kernels: 50.3 us -> 48.2 us
    unnamed x8 -> x2, local copies, waits for them, and re-layouts: 5.37 us -> 1.34 us
    pallas_call x1, Pallas kernels: 50.3 us -> 48.2 us  [body(): pl.pallas_call(functools.partial(kernel, n_sp, n_tp, chunks), out_shape=(...]
where the time goes in v2:
time: 50.3 us; the launch traced here: 50.2 us
  Pallas kernels  48.2 us (96%)
  local copies, waits for them, and re-layouts  1.34 us (3%)
  between operations  0.64 us (1%)
    pallas_call x1, Pallas kernels, body(): pl.pallas_call(functools.partial(kernel, n_sp, n_tp, chunks), out_shape=(...  48.2 us
    unnamed x2, local copies, waits for them, and re-layouts  1.34 us

profile of v2, /device:TPU:0, one launch (start us, length us, event | category | flops | bytes accessed | tf_op | source)
XLA Modules:
  0.0 50.2 jit_solution(15973961148945359209)
XLA Ops:
  0.6 48.2 %attention.1 = (bf16[96,2048]{1,0:T(8,128)(2,1)S(1)}, f32[4,384]{1,0:T(4,128)S(1)}) custom-call(bf16[96,2048]{1,0:T(8,128)(2,1)} %tok_hbm.1, bf16[2048,256]{1,0:T(8,128)(2,1)} %wq_hbm.1, bf16[64,2048]{1,0:T(8,128)(2,1)} %bitcast.2, bf16[64,2048]{1,0:T(8,128)(2,1)} %bitcast.3, bf16[256,2048]{1,0:T(8,128)(2,1)} %wo_hbm.1, bf16[4,64]{1,0:T(4,128)(2,1)} %qg_ref.1, ...), custom_call_target="tpu_custom_call" | custom-call | tf_op jit(solution)/shard_map/attention/pallas_call | solution.py:357
  48.8 0.7 %copy.11 = bf16[96,2048]{1,0:T(8,128)(2,1)} copy(bf16[96,2048]{1,0:T(8,128)(2,1)S(1)} %get-tuple-element.2) | data formatting | bytes 786432
  49.6 0.6 %copy.12 = f32[4,384]{1,0:T(4,128)} copy(f32[4,384]{1,0:T(4,128)S(1)} %get-tuple-element.3) | data formatting | bytes 12288

commit v3 on v1

--- a/solution.py
+++ b/solution.py
@@ -60,8 +60,6 @@
     log_ref,
     tok,
     wq,
-    wk,
-    wv,
     wkv,
     wo,
     gains,
@@ -104,13 +102,11 @@
     def across(i):
         return lax.rem(pair + i, pairs) * 2 + core
 
-    def column(i):
-        return lax.rem(col + i, cols) * 2 + side
-
+    kv_cols = wk_hbm.shape[0]
     loads = [
         pltpu.make_async_copy(src, dst, local_sem.at[i])
         for i, (src, dst) in enumerate(
-            ((tok_hbm, tok.at[tp]), (wq_hbm, wq), (wk_hbm, wk), (wv_hbm, wv), (wo_hbm, wo.at[core]))
+            ((tok_hbm, tok.at[tp]), (wq_hbm, wq), (wk_hbm, wkv.at[0:kv_cols]), (wv_hbm, wkv.at[kv_cols:]), (wo_hbm, wo.at[core]))
         )
     ]
     for load in loads:
@@ -125,7 +121,8 @@
     pl.semaphore_signal(barrier, inc=1, device_id={"sp": other}, device_id_type=MESH)
     peers += 2
     for i in range(1, cols):
-        pl.semaphore_signal(barrier, inc=1, device_id={"sp": column(i)}, device_id_type=MESH)
+        peer = lax.rem(col + i, cols) * 2 + side
+        pl.semaphore_signal(barrier, inc=1, device_id={"sp": peer}, device_id_type=MESH)
         peers += 1
     pl.semaphore_wait(barrier, peers)
 
@@ -161,9 +158,6 @@
     acc[...] = jnp.zeros_like(acc)
     loads[2].wait()
     loads[3].wait()
-    kv_cols = wk.shape[1]
-    wkv[:, 0:kv_cols] = wk[...]
-    wkv[:, kv_cols : 2 * kv_cols] = wv[...]
     loads[1].wait()
     loads[0].wait()
     query_cols = wq.shape[1]
@@ -172,7 +166,9 @@
         piece = tok[block]
         at = pl.ds(pl.multiple_of(block * rows, rows), rows)
         raw[at, 0:query_cols] = jnp.dot(piece, wq[...], preferred_element_type=F32)
-        raw[at, query_cols:] = jnp.dot(piece, wkv[...], preferred_element_type=F32)
+        raw[at, query_cols:] = lax.dot_general(
+            piece, wkv[...], (((1,), (1,)), ((), ())), preferred_element_type=F32
+        )
 
     project(tp)
     token_copy(mate, tok_hbm, 0, mate).wait_recv()
@@ -202,9 +198,23 @@
     def kv_copy(block, slot, where):
         return send(kv.at[block], kv.at[block], kv_send.at[slot], kv_recv.at[block], {"sp": where})
 
-    for i in range(1, cols):
-        go(kv_copy(sp, i, column(i)))
-    go(kv_copy(sp, 0, other))
+    def near(distance, act):
+        for way in (1, -1):
+            place = col + distance * way
+
+            @pl.when(jnp.logical_and(place >= 0, place < cols))
+            def _():
+                act(place)
+
+    def to_column(place):
+        return kv_copy(sp, place, place * 2 + side)
+
+    def to_other(place):
+        return kv_copy(place * 2 + side, cols + place, other)
+
+    to_other(col).start()
+    for distance in range(1, cols):
+        near(distance, lambda place: to_column(place).start())
 
     turned = jnp.transpose(raw[:, 0:query_cols])
     for h in range(heads):
@@ -226,22 +236,30 @@
                 acc[h] = acc[h] * jnp.exp2(old - new) + mixed
                 top[h : h + 1, :] = new
 
+    def straight(place):
+        kv_copy(place * 2 + side, 0, other).wait_recv()
+        to_other(place).start()
+        attend(place * 2 + side)
+
+    def mirrored(place):
+        block = place * 2 + (1 - side)
+        kv_copy(block, 0, other).wait_recv()
+        attend(block)
+
     attend(sp)
-
-    def step(i, carry):
-        block = column(i)
-        kv_copy(block, 0, block).wait_recv()
-        kv_copy(block, cols + i, other).start()
-        attend(block)
-        late = lax.rem(col + i - 1, cols) * 2 + (1 - side)
-        kv_copy(late, 0, other).wait_recv()
-        attend(late)
+    mirrored(col)
+
+    def step(distance, carry):
+        near(distance, straight)
+
+        @pl.when(distance > 1)
+        def _():
+            near(distance - 1, mirrored)
+
         return carry
 
     lax.fori_loop(1, cols, step, 0)
-    late = lax.rem(col + cols - 1, cols) * 2 + (1 - side)
-    kv_copy(late, 0, other).wait_recv()
-    attend(late)
+    near(cols - 1, mirrored)
 
     finished = []
     for h in range(heads):
@@ -298,8 +316,10 @@
         copy.wait_send()
     wo_copy.wait_send()
     att_copy.wait_send()
-    for i in range(1, cols):
-        kv_copy(column(i), cols + i, other).wait_send()
+    to_other(col).wait_send()
+    for distance in range(1, cols):
+        near(distance, lambda place: to_column(place).wait_send())
+        near(distance, lambda place: to_other(place).wait_send())
     for n in range(chunks):
         for i in range(1, pairs):
             part_copy(i, n).wait_send()
@@ -322,17 +342,15 @@
     return pl.pallas_call(
         functools.partial(kernel, n_sp, n_tp, chunks),
         out_shape=(
-            jax.ShapeDtypeStruct((rows, model), BF16),
-            jax.ShapeDtypeStruct((heads, count), F32),
+            pltpu.VMEM((rows, model), BF16),
+            pltpu.VMEM((heads, count), F32),
         ),
         in_specs=[any_space] * 5 + [vmem] * 2,
         out_specs=(vmem, vmem),
         scratch_shapes=[
             pltpu.VMEM((n_tp, rows, depth), BF16),
             pltpu.VMEM((depth, query_cols), BF16),
-            pltpu.VMEM((depth, kv_cols), BF16),
-            pltpu.VMEM((depth, kv_cols), BF16),
-            pltpu.VMEM((depth, 2 * kv_cols), BF16),
+            pltpu.VMEM((2 * kv_cols, depth), BF16),
             pltpu.VMEM((2, group, model), BF16),
             pltpu.VMEM((128, 128), F32),
             pltpu.VMEM((count, query_cols + 2 * kv_cols), F32),
@@ -361,7 +379,7 @@
             collective_id=0, has_side_effects=True, vmem_limit_bytes=60 * 1024 * 1024
         ),
         name="attention",
-    )(tokens, query_weight, key_weight, value_weight, out_weight, query_gain, key_gain)
+    )(tokens, query_weight, key_weight.T, value_weight.T, out_weight, query_gain, key_gain)
 
 
 def solution(mesh):

time: 57.1 us -> 51.3 us (0.90)
  local copies, waits for them, and re-layouts: 5.37 us -> 1.34 us
  Pallas kernels: 50.3 us -> 49.1 us
    unnamed x8 -> x2, local copies, waits for them, and re-layouts: 5.37 us -> 1.34 us
    pallas_call x1, Pallas kernels: 50.3 us -> 49.1 us  [body(): pl.pallas_call(functools.partial(kernel, n_sp, n_tp, chunks), out_shape=(...]
where the time goes in v3:
time: 51.3 us; the launch traced here: 51.1 us
  Pallas kernels  49.1 us (96%)
  local copies, waits for them, and re-layouts  1.34 us (3%)
  between operations  0.64 us (1%)
    pallas_call x1, Pallas kernels, body(): pl.pallas_call(functools.partial(kernel, n_sp, n_tp, chunks), out_shape=(...  49.1 us
    unnamed x2, local copies, waits for them, and re-layouts  1.34 us

profile of v3, /device:TPU:0, one launch (start us, length us, event | category | flops | bytes accessed | tf_op | source)
XLA Modules:
  0.0 51.1 jit_solution(4369496616868452999)
XLA Ops:
  0.6 49.1 %attention.1 = (bf16[96,2048]{1,0:T(8,128)(2,1)S(1)}, f32[4,384]{1,0:T(4,128)S(1)}) custom-call(bf16[96,2048]{1,0:T(8,128)(2,1)} %tok_hbm.1, bf16[2048,256]{1,0:T(8,128)(2,1)} %wq_hbm.1, bf16[64,2048]{1,0:T(8,128)(2,1)} %bitcast.2, bf16[64,2048]{1,0:T(8,128)(2,1)} %bitcast.3, bf16[256,2048]{1,0:T(8,128)(2,1)} %wo_hbm.1, bf16[4,64]{1,0:T(4,128)(2,1)} %qg_ref.1, ...), custom_call_target="tpu_custom_call" | custom-call | tf_op jit(solution)/shard_map/attention/pallas_call | solution.py:342
  49.8 0.7 %copy.11 = bf16[96,2048]{1,0:T(8,128)(2,1)} copy(bf16[96,2048]{1,0:T(8,128)(2,1)S(1)} %get-tuple-element.2) | data formatting | bytes 786432
  50.5 0.6 %copy.12 = f32[4,384]{1,0:T(4,128)} copy(f32[4,384]{1,0:T(4,128)S(1)} %get-tuple-element.3) | data formatting | bytes 12288

commit v4 on v3

--- a/solution.py
+++ b/solution.py
@@ -170,9 +170,54 @@
             piece, wkv[...], (((1,), (1,)), ((), ())), preferred_element_type=F32
         )
 
+    kv_rows = kv_heads * width
+    span = 2 * rows
+
+    def span_of(part):
+        return pl.ds(pl.multiple_of(part * span, span), span)
+
+    def make_kv(part):
+        at = span_of(part)
+        turned = jnp.transpose(raw[at, query_cols : query_cols + kv_rows])
+        angles = angle_tables(sp * count + part * span, span, width // 4)
+        for h in range(kv_heads):
+            gain = turned_gains[0:width, heads + h : heads + h + 1]
+            keys = prepare(turned[h * width : (h + 1) * width], gain, angles)
+            kv[sp, at, h * width : (h + 1) * width] = jnp.transpose(keys).astype(BF16)
+        kv[sp, at, kv_rows : 2 * kv_rows] = raw[at, query_cols + kv_rows :].astype(BF16)
+
+    def kv_copy(block, part, slot, where):
+        spot = kv.at[block, span_of(part)]
+        return send(spot, spot, kv_send.at[slot, part], kv_recv.at[block, part], {"sp": where})
+
+    def near(distance, act):
+        for way in (1, -1):
+            place = col + distance * way
+
+            @pl.when(jnp.logical_and(place >= 0, place < cols))
+            def _():
+                act(place)
+
+    def to_column(place, part):
+        return kv_copy(sp, part, place, place * 2 + side)
+
+    def to_other(place, part):
+        return kv_copy(place * 2 + side, part, cols + place, other)
+
+    def send_kv(part):
+        to_other(col, part).start()
+        for distance in range(1, cols):
+            near(distance, lambda place: to_column(place, part).start())
+
+    def forward(place, part):
+        kv_copy(place * 2 + side, part, 0, other).wait_recv()
+        to_other(place, part).start()
+
     project(tp)
     token_copy(mate, tok_hbm, 0, mate).wait_recv()
     project(mate)
+    make_kv(pair)
+    send_kv(pair)
     for i in range(1, pairs):
         block = across(i)
         token_copy(block, tok_hbm, i, block).wait_recv()
@@ -185,36 +230,11 @@
         block = lax.rem(pair + i, pairs) * 2 + (1 - core)
         token_copy(block, tok_hbm, i, mate).wait_recv()
         project(block)
-
-    turned = jnp.transpose(raw[:, query_cols:])
-    kv_rows = kv_heads * width
-    for h in range(kv_heads):
-        keys = prepare(
-            turned[h * width : (h + 1) * width], turned_gains[0:width, heads + h : heads + h + 1], tables
-        )
-        kv[sp, h * width : (h + 1) * width, :] = keys.astype(BF16)
-    kv[sp, kv_rows : 2 * kv_rows, :] = turned[kv_rows : 2 * kv_rows].astype(BF16)
-
-    def kv_copy(block, slot, where):
-        return send(kv.at[block], kv.at[block], kv_send.at[slot], kv_recv.at[block], {"sp": where})
-
-    def near(distance, act):
-        for way in (1, -1):
-            place = col + distance * way
-
-            @pl.when(jnp.logical_and(place >= 0, place < cols))
-            def _():
-                act(place)
-
-    def to_column(place):
-        return kv_copy(sp, place, place * 2 + side)
-
-    def to_other(place):
-        return kv_copy(place * 2 + side, cols + place, other)
-
-    to_other(col).start()
+        part = lax.rem(pair + i, pairs)
+        make_kv(part)
+        send_kv(part)
     for distance in range(1, cols):
-        near(distance, lambda place: to_column(place).start())
+        near(distance, lambda place: forward(place, pair))
 
     turned = jnp.transpose(raw[:, 0:query_cols])
     for h in range(heads):
@@ -223,9 +243,10 @@
 
     def attend(block):
         ones = jnp.ones((ONES, count), BF16)
+        turned = jnp.transpose(kv[block])
         for g in range(kv_heads):
-            keys = jnp.transpose(kv[block, g * width : (g + 1) * width, :])
-            values = kv[block, kv_rows + g * width : kv_rows + (g + 1) * width, :]
+            keys = kv[block, :, g * width : (g + 1) * width]
+            values = turned[kv_rows + g * width : kv_rows + (g + 1) * width]
             values = jnp.concatenate([values, ones], axis=0)
             for h in range(g * share, (g + 1) * share):
                 scores = jnp.dot(keys, queries[h], preferred_element_type=F32)
@@ -237,13 +258,14 @@
                 top[h : h + 1, :] = new
 
     def straight(place):
-        kv_copy(place * 2 + side, 0, other).wait_recv()
-        to_other(place).start()
+        for i in range(1, pairs):
+            forward(place, lax.rem(pair + i, pairs))
         attend(place * 2 + side)
 
     def mirrored(place):
         block = place * 2 + (1 - side)
-        kv_copy(block, 0, other).wait_recv()
+        for part in range(pairs):
+            kv_copy(block, part, 0, other).wait_recv()
         attend(block)
 
     attend(sp)
@@ -316,10 +338,11 @@
         copy.wait_send()
     wo_copy.wait_send()
     att_copy.wait_send()
-    to_other(col).wait_send()
-    for distance in range(1, cols):
-        near(distance, lambda place: to_column(place).wait_send())
-        near(distance, lambda place: to_other(place).wait_send())
+    for part in range(pairs):
+        to_other(col, part).wait_send()
+        for distance in range(1, cols):
+            near(distance, lambda place: to_column(place, part).wait_send())
+            near(distance, lambda place: to_other(place, part).wait_send())
     for n in range(chunks):
         for i in range(1, pairs):
             part_copy(i, n).wait_send()
@@ -355,7 +378,7 @@
             pltpu.VMEM((128, 128), F32),
             pltpu.VMEM((count, query_cols + 2 * kv_cols), F32),
             pltpu.VMEM((heads, width, count), BF16),
-            pltpu.VMEM((n_sp, 2 * kv_heads * width, count), BF16),
+            pltpu.VMEM((n_sp, count, 2 * kv_heads * width), BF16),
             pltpu.VMEM((heads, count), F32),
             pltpu.VMEM((heads, width + ONES, count), F32),
             pltpu.VMEM((pairs, rows, group), BF16),
@@ -368,8 +391,8 @@
             dma((n_tp,)),
             dma,
             dma,
-            dma((2 * cols,)),
-            dma((n_sp,)),
+            dma((2 * cols, pairs)),
+            dma((n_sp, pairs)),
             dma,
             dma,
             dma((slots,)),

time: 51.3 us -> 46.7 us (0.910)
  Pallas kernels: 49.1 us -> 44.5 us
    pallas_call x1, Pallas kernels: 49.1 us -> 44.5 us  [body(): pl.pallas_call(functools.partial(kernel, n_sp, n_tp, chunks), out_shape=(...]
where the time goes in v4:
time: 46.7 us; the launch traced here: 46.5 us
  Pallas kernels  44.5 us (95%)
  local copies, waits for them, and re-layouts  1.34 us (3%)
  between operations  0.64 us (1%)
    pallas_call x1, Pallas kernels, body(): pl.pallas_call(functools.partial(kernel, n_sp, n_tp, chunks), out_shape=(...  44.5 us
    unnamed x2, local copies, waits for them, and re-layouts  1.34 us

profile of v4, /device:TPU:0, one launch (start us, length us, event | category | flops | bytes accessed | tf_op | source)
XLA Modules:
  0.0 46.5 jit_solution(2759891391099343596)
XLA Ops:
  0.6 44.5 %attention.1 = (bf16[96,2048]{1,0:T(8,128)(2,1)S(1)}, f32[4,384]{1,0:T(4,128)S(1)}) custom-call(bf16[96,2048]{1,0:T(8,128)(2,1)} %tok_hbm.1, bf16[2048,256]{1,0:T(8,128)(2,1)} %wq_hbm.1, bf16[64,2048]{1,0:T(8,128)(2,1)} %bitcast.2, bf16[64,2048]{1,0:T(8,128)(2,1)} %bitcast.3, bf16[256,2048]{1,0:T(8,128)(2,1)} %wo_hbm.1, bf16[4,64]{1,0:T(4,128)(2,1)} %qg_ref.1, ...), custom_call_target="tpu_custom_call" | custom-call | tf_op jit(solution)/shard_map/attention/pallas_call | solution.py:365
  45.2 0.7 %copy.11 = bf16[96,2048]{1,0:T(8,128)(2,1)} copy(bf16[96,2048]{1,0:T(8,128)(2,1)S(1)} %get-tuple-element.2) | data formatting | bytes 786432
  45.9 0.6 %copy.12 = f32[4,384]{1,0:T(4,128)} copy(f32[4,384]{1,0:T(4,128)S(1)} %get-tuple-element.3) | data formatting | bytes 12288

commit v5 on v4

--- a/solution.py
+++ b/solution.py
@@ -252,7 +252,7 @@
                 scores = jnp.dot(keys, queries[h], preferred_element_type=F32)
                 old = top[h : h + 1, :]
                 new = jnp.maximum(old, jnp.max(scores, axis=0, keepdims=True))
-                weights = jnp.exp2(scores - new).astype(BF16)
+                weights = jnp.exp2((scores - new).astype(BF16))
                 mixed = jnp.dot(values, weights, preferred_element_type=F32)
                 acc[h] = acc[h] * jnp.exp2(old - new) + mixed
                 top[h : h + 1, :] = new

time: 46.7 us -> 46.9 us (level)
  no operation moved by 1% of the time
where the time goes in v5:
time: 46.9 us; the launch traced here: 46.7 us
  Pallas kernels  44.7 us (95%)
  local copies, waits for them, and re-layouts  1.34 us (3%)
  between operations  0.64 us (1%)
    pallas_call x1, Pallas kernels, body(): pl.pallas_call(functools.partial(kernel, n_sp, n_tp, chunks), out_shape=(...  44.7 us
    unnamed x2, local copies, waits for them, and re-layouts  1.34 us

profile of v5, /device:TPU:0, one launch (start us, length us, event | category | flops | bytes accessed | tf_op | source)
XLA Modules:
  0.0 46.7 jit_solution(8689764137780600745)
XLA Ops:
  0.6 44.7 %attention.1 = (bf16[96,2048]{1,0:T(8,128)(2,1)S(1)}, f32[4,384]{1,0:T(4,128)S(1)}) custom-call(bf16[96,2048]{1,0:T(8,128)(2,1)} %tok_hbm.1, bf16[2048,256]{1,0:T(8,128)(2,1)} %wq_hbm.1, bf16[64,2048]{1,0:T(8,128)(2,1)} %bitcast.2, bf16[64,2048]{1,0:T(8,128)(2,1)} %bitcast.3, bf16[256,2048]{1,0:T(8,128)(2,1)} %wo_hbm.1, bf16[4,64]{1,0:T(4,128)(2,1)} %qg_ref.1, ...), custom_call_target="tpu_custom_call" | custom-call | tf_op jit(solution)/shard_map/attention/pallas_call | solution.py:365
  45.4 0.7 %copy.11 = bf16[96,2048]{1,0:T(8,128)(2,1)} copy(bf16[96,2048]{1,0:T(8,128)(2,1)S(1)} %get-tuple-element.2) | data formatting | bytes 786432
  46.1 0.6 %copy.12 = f32[4,384]{1,0:T(4,128)} copy(f32[4,384]{1,0:T(4,128)S(1)} %get-tuple-element.3) | data formatting | bytes 12288
